TPU v7x, 32 devices: a whole 2x2x4 slice. The times are simulated.
32 devices in a mesh: kv: 8 (over z, core), tp: 4 (over y, x).
Axes of the slice: x: 2, y: 2, z: 4, core: 2. Of those that a mesh axis runs over, the one named last changes fastest.
Arguments:
- tokens: bfloat16 [64, 4096], P(None, ('kv', 'tp')), may hold values from -3 to 3
- lengths: int32 [16], replicated, may hold values from 1 to 4, 32 in all
- states: float32 [16, 16, 128, 128], P('kv', 'tp'), may hold values from -3 to 3
- gain_pre: float32 [4096], P('kv'), may hold values from 0.1 to 1.9
- pre_gate: bfloat16 [4096, 11264], P('kv', 'tp'), may hold values from -0.09375 to 0.09375
- pre_up: bfloat16 [4096, 11264], P('kv', 'tp'), may hold values from -0.09375 to 0.09375
- pre_down: bfloat16 [11264, 4096], P('tp', 'kv'), may hold values from -1 to 1
- gain_mix: float32 [4096], P('kv'), may hold values from 0.1 to 1.9
- query_weight: bfloat16 [4096, 2048], P('kv', 'tp'), may hold values from -0.09375 to 0.09375
- forget_weight: bfloat16 [4096, 2048], P('kv', 'tp'), may hold values from -0.09375 to 0.09375
- input_weight: bfloat16 [4096, 2048], P('kv', 'tp'), may hold values from -0.09375 to 0.09375
- outgate_weight: bfloat16 [4096, 2048], P('kv', 'tp'), may hold values from -0.09375 to 0.09375
- forget_floor: float32 [2048], P('tp'), may hold values from 0 to 0.9
- head_gain: float32 [128], replicated, may hold values from 0.1 to 1.9
- mix_weight: bfloat16 [2048, 4096], P('tp', 'kv'), may hold values from -1 to 1
- gain_post: float32 [4096], P('kv'), may hold values from 0.1 to 1.9
- post_gate: bfloat16 [4096, 11264], P('kv', 'tp'), may hold values from -0.09375 to 0.09375
- post_up: bfloat16 [4096, 11264], P('kv', 'tp'), may hold values from -0.09375 to 0.09375
- post_down: bfloat16 [11264, 4096], P('tp', 'kv'), may hold values from -0.0546875 to 0.0546875
Outputs:
- out_tokens: bfloat16 [64, 4096], P(None, ('kv', 'tp'))
- new_states: float32 [16, 16, 128, 128], P('kv', 'tp')
Inputs may be any that keep to these rules, and one draw needn't show every extreme that they name: `lengths`: each of the 16 sequences has 1 to 4 new tokens, 32 in all, and at least one has exactly 4.
All inputs are finite; a program needn't handle non-finite values.
Results may differ from a plain program's by a relative error of at most 0.011.
Values may be sent and summed in bfloat16 or wider, within the bound.
A program may use at most 64 MiB of HBM per device.

v0:
```python
import jax
import jax.numpy as jnp
from jax import lax
from jax.sharding import PartitionSpec as P

D = 4096
DK = 128
W = 4
EPSILON = 1e-06


def gathered_norm(shard, gain_block):
    gathered = lax.all_gather(shard, "tp", axis=1, tiled=True)
    block_squares = jnp.sum(jnp.square(gathered.astype(jnp.float32)), axis=1)
    totals = lax.psum(block_squares, "kv")
    scale = lax.rsqrt(totals[:, None] / D + EPSILON)
    return (gathered.astype(jnp.float32) * scale * gain_block).astype(jnp.bfloat16)


def half_mixer(shard, gain_block, gate_weight, up_weight, down_weight):
    normed = gathered_norm(shard, gain_block)
    half_cols = gate_weight.shape[1]
    owned = lax.psum_scatter(
        jnp.concatenate(
            [
                jnp.dot(normed, gate_weight, preferred_element_type=jnp.float32),
                jnp.dot(normed, up_weight, preferred_element_type=jnp.float32),
            ],
            axis=1,
        ),
        "kv",
        scatter_dimension=0,
        tiled=True,
    )
    hidden = (jax.nn.silu(owned[:, :half_cols]) * owned[:, half_cols:]).astype(jnp.bfloat16)
    partial_out = jnp.dot(
        lax.all_gather(hidden, "kv", axis=0, tiled=True),
        down_weight,
        preferred_element_type=jnp.float32,
    )
    return lax.psum_scatter(partial_out, "tp", scatter_dimension=1, tiled=True)


def local(
    tokens,
    lengths,
    states,
    gain_pre,
    pre_gate,
    pre_up,
    pre_down,
    gain_mix,
    query_weight,
    forget_weight,
    input_weight,
    outgate_weight,
    forget_floor,
    head_gain,
    mix_weight,
    gain_post,
    post_gate,
    post_up,
    post_down,
):
    resid_one = (
        tokens.astype(jnp.float32) + 0.5 * half_mixer(tokens, gain_pre, pre_gate, pre_up, pre_down)
    ).astype(jnp.bfloat16)
    normed = gathered_norm(resid_one, gain_mix)
    head_cols = query_weight.shape[1]
    seq_local = states.shape[0]
    heads_local = states.shape[1]
    owned = lax.psum_scatter(
        jnp.concatenate(
            [
                jnp.dot(normed, query_weight, preferred_element_type=jnp.float32),
                jnp.dot(normed, forget_weight, preferred_element_type=jnp.float32),
                jnp.dot(normed, input_weight, preferred_element_type=jnp.float32),
                jnp.dot(normed, outgate_weight, preferred_element_type=jnp.float32),
            ],
            axis=1,
        ),
        "kv",
        scatter_dimension=0,
        tiled=True,
    )
    shape_four = (seq_local, W, heads_local, DK)
    queries = jax.nn.silu(owned[:, :head_cols]).reshape(shape_four)
    forget_raw = owned[:, head_cols : 2 * head_cols].reshape(shape_four)
    fresh_values = owned[:, 2 * head_cols : 3 * head_cols].reshape(shape_four)
    gating = owned[:, 3 * head_cols :].reshape(shape_four)
    local_lengths = lax.dynamic_slice_in_dim(lengths, lax.axis_index("kv") * seq_local, seq_local)
    live_mask = jnp.arange(W, dtype=jnp.int32)[None, :] < local_lengths[:, None]
    live_four = live_mask[:, :, None, None]
    floors = forget_floor.reshape(heads_local, DK)
    forgets = jnp.where(
        live_four, floors + (1.0 - floors) * jax.nn.sigmoid(forget_raw), jnp.float32(1.0)
    )
    write_rate = 1.0 - forgets
    carried = states
    readings = []
    for offset in range(W):
        carried = (
            forgets[:, offset, :, :, None] * carried
            + write_rate[:, offset, :, :, None] * fresh_values[:, offset, :, None, :]
        )
        readings.append(
            jnp.einsum(
                "bhk,bhkv->bhv", queries[:, offset], carried, precision=lax.Precision.HIGHEST
            )
        )
    read_out = jnp.stack(readings, axis=1)
    meansq = jnp.mean(read_out * read_out, axis=3, keepdims=True)
    head_out = (
        (
            read_out
            * lax.rsqrt(meansq + EPSILON)
            * head_gain
            * jax.nn.silu(gating)
            * live_four.astype(jnp.float32)
        )
        .astype(jnp.bfloat16)
        .reshape(seq_local * W, heads_local * DK)
    )
    mixed_part = jnp.dot(
        lax.all_gather(head_out, "kv", axis=0, tiled=True),
        mix_weight,
        preferred_element_type=jnp.float32,
    )
    mixed = lax.psum_scatter(mixed_part, "tp", scatter_dimension=1, tiled=True)
    resid_two = (resid_one.astype(jnp.float32) + mixed).astype(jnp.bfloat16)
    finished = resid_two.astype(jnp.float32) + 0.5 * half_mixer(
        resid_two, gain_post, post_gate, post_up, post_down
    )
    live_rows = (
        (jnp.arange(W, dtype=jnp.int32)[None, :] < lengths[:, None])
        .reshape(-1, 1)
        .astype(jnp.float32)
    )
    outcome = (finished * live_rows).astype(jnp.bfloat16)
    return (outcome, carried)


def solution(mesh):
    placed = (
        P(None, ("kv", "tp")),
        P(),
        P("kv", "tp", None, None),
        P("kv"),
        P("kv", "tp"),
        P("kv", "tp"),
        P("tp", "kv"),
        P("kv"),
        P("kv", "tp"),
        P("kv", "tp"),
        P("kv", "tp"),
        P("kv", "tp"),
        P("tp"),
        P(),
        P("tp", "kv"),
        P("kv"),
        P("kv", "tp"),
        P("kv", "tp"),
        P("tp", "kv"),
    )
    return jax.shard_map(
        local,
        mesh=mesh,
        in_specs=placed,
        out_specs=(P(None, ("kv", "tp")), P("kv", "tp", None, None)),
        check_vma=False,
    )
```

profile of v0, /device:TPU:0, one launch (start us, length us, event | category | flops | bytes accessed | tf_op | source)
XLA Modules:
  0.0 318.7 jit_solution(17917307360592700447)
XLA Ops:
  7.2 10.1 %all_gather.18 = bf16[64,512]{1,0:T(8,128)(2,1)S(1)} all-gather(bf16[64,128]{1,0:T(8,128)(2,1)} %param.19), channel_id=1, replica_groups=mesh['kv'=8,'tp'=4] {'tp'}, dimensions={1}, use_global_device_ids=true | all-gather | bytes 81920 | tf_op jit(solution)/shard_map/all_gather | solution.py:13
  17.3 0.1 fusion.8
  17.5 14.9 %psum.21 = f32[64]{0:T(128)S(1)} all-reduce(f32[64]{0:T(128)S(1)} %fusion.8), channel_id=1, replica_groups=mesh['kv'=8,'tp'=4] {'kv'}, use_global_device_ids=true, to_apply=%region_1.0 | all-reduce | flops 64 | bytes 512 | tf_op jit(solution)/shard_map/psum | solution.py:15
  32.4 1.5 fusion.26
  33.9 0.3 copy-done.1
  34.2 0.7 fusion.24
  34.8 1.2 pad_maximum_fusion
  36.1 31.3 %reduce-scatter.7.cloned.1.call-done = f32[8,5632]{1,0:T(8,128)} async-done(((f32[64,5632]{1,0:T(8,128)}), f32[8,5632]{1,0:T(8,128)}) %reduce-scatter.7.cloned.1.call-update) | async-done | bytes 180240 | tf_op jit(solution)/shard_map/reduce_scatter | solution.py:23
  67.4 1.0 fusion.19
  68.4 14.4 %all_gather.19 = bf16[64,2816]{1,0:T(8,128)(2,1)S(1)} all-gather(bf16[8,2816]{1,0:T(8,128)(2,1)S(1)} %fusion.19), channel_id=1, replica_groups=mesh['kv'=8,'tp'=4] {'kv'}, dimensions={0}, use_global_device_ids=true | all-gather | bytes 405504 | tf_op jit(solution)/shard_map/all_gather | solution.py:37
  82.7 3.1 fusion.45
  85.9 22.2 %reduce-scatter.9.cloned.1.call-done = f32[64,128]{1,0:T(8,128)} async-done(((f32[64,512]{1,0:T(8,128)}), f32[64,128]{1,0:T(8,128)}) %reduce-scatter.9.cloned.1.call-update) | async-done | bytes 32784 | tf_op jit(solution)/shard_map/reduce_scatter | solution.py:41
  108.1 0.8 add_convert_fusion.1
  108.8 8.1 %all_gather.20 = bf16[64,512]{1,0:T(8,128)(2,1)S(1)} all-gather(bf16[64,128]{1,0:T(8,128)(2,1)S(1)} %add_convert_fusion.1), channel_id=1, replica_groups=mesh['kv'=8,'tp'=4] {'tp'}, dimensions={1}, use_global_device_ids=true | all-gather | bytes 81920 | tf_op jit(solution)/shard_map/all_gather | solution.py:13
  117.0 0.1 fusion.11
  117.1 13.9 %psum.22 = f32[64]{0:T(128)S(1)} all-reduce(f32[64]{0:T(128)S(1)} %fusion.11), channel_id=1, replica_groups=mesh['kv'=8,'tp'=4] {'kv'}, use_global_device_ids=true, to_apply=%region_5.6 | all-reduce | flops 64 | bytes 512 | tf_op jit(solution)/shard_map/psum | solution.py:15
  131.0 1.3 fusion.42
  132.3 1.3 fusion.40
  133.6 1.3 fusion.38
  134.9 1.3 fusion.36
  136.2 0.8 pad_maximum_fusion.2
  137.3 28.2 %reduce-scatter.11.cloned.1.call-done = f32[8,2048]{1,0:T(8,128)} async-done(((f32[64,2048]{1,0:T(8,128)}), f32[8,2048]{1,0:T(8,128)}) %reduce-scatter.11.cloned.1.call-update) | async-done | bytes 65552 | tf_op jit(solution)/shard_map/reduce_scatter | solution.py:72
  165.6 0.8 fusion.33
  166.5 0.8 fusion
  167.3 1.1 fusion.17
  168.4 1.5 fusion.1
  169.9 1.3 multiply_add_fusion
  171.2 0.8 copy-done.4
  172.0 0.5 fusion.46
  172.5 0.1 multiply_reduce_fusion
  172.7 0.8 fusion.30
  173.5 14.0 %all_gather.21 = bf16[64,512]{1,0:T(8,128)(2,1)S(1)} all-gather(bf16[8,512]{1,0:T(8,128)(2,1)S(1)} %fusion.30), channel_id=1, replica_groups=mesh['kv'=8,'tp'=4] {'kv'}, dimensions={0}, use_global_device_ids=true | all-gather | bytes 73728 | tf_op jit(solution)/shard_map/all_gather | solution.py:125
  187.5 0.8 fusion.47
  188.4 22.4 %reduce-scatter.13.cloned.1.call-done = f32[64,128]{1,0:T(8,128)} async-done(((f32[64,512]{1,0:T(8,128)}), f32[64,128]{1,0:T(8,128)}) %reduce-scatter.13.cloned.1.call-update) | async-done | bytes 32784 | tf_op jit(solution)/shard_map/reduce_scatter | solution.py:129
  210.8 0.8 add_convert_fusion
  211.5 8.2 %all_gather.22 = bf16[64,512]{1,0:T(8,128)(2,1)S(1)} all-gather(bf16[64,128]{1,0:T(8,128)(2,1)S(1)} %add_convert_fusion), channel_id=1, replica_groups=mesh['kv'=8,'tp'=4] {'tp'}, dimensions={1}, use_global_device_ids=true | all-gather | bytes 81920 | tf_op jit(solution)/shard_map/all_gather | solution.py:13
  219.7 0.1 fusion.14
  219.8 13.9 %psum.23 = f32[64]{0:T(128)S(1)} all-reduce(f32[64]{0:T(128)S(1)} %fusion.14), channel_id=1, replica_groups=mesh['kv'=8,'tp'=4] {'kv'}, use_global_device_ids=true, to_apply=%region_10.11 | all-reduce | flops 64 | bytes 512 | tf_op jit(solution)/shard_map/psum | solution.py:15
  233.7 2.6 fusion.22
  236.4 0.7 fusion.20
  237.0 1.2 pad_maximum_fusion.1
  238.3 31.2 %reduce-scatter.15.cloned.1.call-done = f32[8,5632]{1,0:T(8,128)} async-done(((f32[64,5632]{1,0:T(8,128)}), f32[8,5632]{1,0:T(8,128)}) %reduce-scatter.15.cloned.1.call-update) | async-done | bytes 180240 | tf_op jit(solution)/shard_map/reduce_scatter | solution.py:23
  269.6 1.0 fusion.18
  270.5 14.4 %all_gather.23 = bf16[64,2816]{1,0:T(8,128)(2,1)S(1)} all-gather(bf16[8,2816]{1,0:T(8,128)(2,1)S(1)} %fusion.18), channel_id=1, replica_groups=mesh['kv'=8,'tp'=4] {'kv'}, dimensions={0}, use_global_device_ids=true | all-gather | bytes 405504 | tf_op jit(solution)/shard_map/all_gather | solution.py:37
  284.9 3.1 fusion.48
  288.1 0.1 reshape.130
  288.1 22.2 %reduce-scatter.17.cloned.1.call-done = f32[64,128]{1,0:T(8,128)} async-done(((f32[64,512]{1,0:T(8,128)}), f32[64,128]{1,0:T(8,128)}) %reduce-scatter.17.cloned.1.call-update) | async-done | bytes 32784 | tf_op jit(solution)/shard_map/reduce_scatter | solution.py:41
  310.4 1.4 multiply_convert_fusion
  (54 shorter events, 1.0 us)
Async XLA Ops:
  7.2 25.2 %copy-start = (bf16[512,2816]{1,0:T(8,128)(2,1)S(1)}, bf16[512,2816]{1,0:T(8,128)(2,1)}, u32[]{:S(2)}) copy-start(bf16[512,2816]{1,0:T(8,128)(2,1)} %param.23) | copy-start | bytes 8650756
  7.2 26.7 %copy-start.8 = (f32[512]{0:T(512)S(1)}, f32[512]{0:T(512)}, u32[]{:S(2)}) copy-start(f32[512]{0:T(512)} %param.22) | copy-start | bytes 6148
  7.2 60.2 %reduce-scatter.7.cloned.1.call-start = ((), (), s32[]{:S(2)}) async-start(), calls=%async_computation.6 | async-start | bytes 1622016 | tf_op jit(solution)/shard_map/reduce_scatter | solution.py:23
  32.3 1.8 copy-start.1
  36.1 72.0 %copy-start.6 = (bf16[64,128]{1,0:T(8,128)(2,1)S(1)}, bf16[64,128]{1,0:T(8,128)(2,1)}, u32[]{:S(2)}) copy-start(bf16[64,128]{1,0:T(8,128)(2,1)} %param.19) | copy-start | bytes 49156
  36.1 94.9 %copy-start.7 = (f32[512]{0:T(512)S(1)}, f32[512]{0:T(512)}, u32[]{:S(2)}) copy-start(f32[512]{0:T(512)} %param.26) | copy-start | bytes 6148
  36.1 72.0 %reduce-scatter.9.cloned.1.call-start = ((), (), s32[]{:S(2)}) async-start(), calls=%async_computation.7 | async-start | bytes 163840 | tf_op jit(solution)/shard_map/reduce_scatter | solution.py:41
  85.8 51.2 %copy-start.12 = (s32[16]{0:T(128)S(1)}, s32[16]{0:T(128)}, u32[]{:S(2)}) copy-start(s32[16]{0:T(128)} %param.20) | copy-start | bytes 196
  85.8 51.5 %copy-start.11 = (f32[128]{0:T(128)S(1)}, f32[128]{0:T(128)}, u32[]{:S(2)}) copy-start(f32[128]{0:T(128)} %param.32) | copy-start | bytes 1540
  85.8 51.5 %copy-start.10 = (f32[512]{0:T(512)S(1)}, f32[512]{0:T(512)}, u32[]{:S(2)}) copy-start(f32[512]{0:T(512)} %param.31) | copy-start | bytes 6148
  85.8 80.7 %copy-start.3 = (f32[2,4,128,128]{3,2,1,0:T(8,128)S(1)}, f32[2,4,128,128]{3,2,1,0:T(8,128)}, u32[]{:S(2)}) copy-start(f32[2,4,128,128]{3,2,1,0:T(8,128)} %param.21) | copy-start | bytes 1572868
  85.9 79.7 %reduce-scatter.11.cloned.1.call-start = ((), (), s32[]{:S(2)}) async-start(), calls=%async_computation.8 | async-start | bytes 589824 | tf_op jit(solution)/shard_map/reduce_scatter | solution.py:72
  137.0 73.8 %reduce-scatter.13.cloned.1.call-start = ((), (), s32[]{:S(2)}) async-start(), calls=%async_computation.9 | async-start | bytes 163840 | tf_op jit(solution)/shard_map/reduce_scatter | solution.py:129
  166.4 21.1 %copy-start.5 = (bf16[512,512]{1,0:T(8,128)(2,1)S(1)}, bf16[512,512]{1,0:T(8,128)(2,1)}, u32[]{:S(2)}) copy-start(bf16[512,512]{1,0:T(8,128)(2,1)} %param.33) | copy-start | bytes 1572868
  166.5 67.2 %copy-start.9 = (f32[512]{0:T(512)S(1)}, f32[512]{0:T(512)}, u32[]{:S(2)}) copy-start(f32[512]{0:T(512)} %param.34) | copy-start | bytes 6148
  171.2 0.8 copy-start.4
  188.3 81.2 %reduce-scatter.15.cloned.1.call-start = ((), (), s32[]{:S(2)}) async-start(), calls=%async_computation.10 | async-start | bytes 1622016 | tf_op jit(solution)/shard_map/reduce_scatter | solution.py:23
  233.7 2.7 copy-start.2
  238.3 72.1 %reduce-scatter.17.cloned.1.call-start = ((), (), s32[]{:S(2)}) async-start(), calls=%async_computation.11 | async-start | bytes 163840 | tf_op jit(solution)/shard_map/reduce_scatter | solution.py:41
Sparse Core Ops, SparseCore 0:
  36.2 31.1 reduce-scatter.6
  86.0 22.0 reduce-scatter.8
  137.1 28.3 reduce-scatter.10
  188.4 22.2 reduce-scatter.12
  238.4 31.1 reduce-scatter.14
  288.1 22.2 reduce-scatter.16
where the time goes:
time: 320 us; the launch traced here: 319 us
  waiting for transfers between devices  158 us (49%)
  blocking collectives  112 us (35%)
  matrix products  21.5 us (7%)
  between operations  14.3 us (4%)
  other arithmetic  11.7 us (4%)
    reduce_scatter x2, waiting for transfers between devices, half_mixer(): lax.psum_scatter(jnp.concatenate([jnp.dot(normed, gate_weight, preferred_...  62.5 us
    reduce_scatter x2, waiting for transfers between devices, half_mixer(): return lax.psum_scatter(partial_out, 'tp', scatter_dimension=1, tiled=True)  44.4 us
    psum x3, blocking collectives, gathered_norm(): totals = lax.psum(block_squares, 'kv')  42.6 us
    all_gather x2, blocking collectives, half_mixer(): lax.all_gather(hidden, 'kv', axis=0, tiled=True)  28.7 us
    reduce_scatter x1, waiting for transfers between devices, local(): lax.psum_scatter(jnp.concatenate([jnp.dot(normed, query_weight, preferred...  28.2 us
    all_gather x3, blocking collectives, gathered_norm(): gathered = lax.all_gather(shard, 'tp', axis=1, tiled=True)  26.4 us
    reduce_scatter x1, waiting for transfers between devices, local(): mixed = lax.psum_scatter(mixed_part, 'tp', scatter_dimension=1, tiled=True)  22.4 us
    all_gather x1, blocking collectives, local(): lax.all_gather(head_out, 'kv', axis=0, tiled=True)  14 us
  transfers between devices with their start and end apart: 6, of which 6 were waited for; matrix products, arithmetic and copies ran while one was open for 0% of the time, Pallas kernels for 0%

commit v1 on v0

--- a/solution.py
+++ b/solution.py
@@ -12,7 +12,7 @@
 def gathered_norm(shard, gain_block):
     gathered = lax.all_gather(shard, "tp", axis=1, tiled=True)
     block_squares = jnp.sum(jnp.square(gathered.astype(jnp.float32)), axis=1)
-    totals = lax.psum(block_squares, "kv")
+    totals = jnp.sum(lax.all_gather(block_squares, "kv"), axis=0)
     scale = lax.rsqrt(totals[:, None] / D + EPSILON)
     return (gathered.astype(jnp.float32) * scale * gain_block).astype(jnp.bfloat16)
 

time: 320 us -> 323 us (level)
    psum x3 -> x0, blocking collectives: 42.6 us -> none  [gathered_norm(): totals = lax.psum(block_squares, 'kv')]
    unnamed x0 -> x3, blocking collectives: none -> 42.6 us
where the time goes in v1:
time: 323 us; the launch traced here: 322 us
  waiting for transfers between devices  158 us (49%)
  blocking collectives  112 us (35%)
  matrix products  21.5 us (7%)
  between operations  15 us (5%)
  other arithmetic  11.8 us (4%)
  local copies, waits for them, and re-layouts  3.68 us (1%)
    reduce_scatter x2, waiting for transfers between devices, half_mixer(): lax.psum_scatter(jnp.concatenate([jnp.dot(normed, gate_weight, preferred_...  62.5 us
    reduce_scatter x2, waiting for transfers between devices, half_mixer(): return lax.psum_scatter(partial_out, 'tp', scatter_dimension=1, tiled=True)  44.5 us
    unnamed x3, blocking collectives  42.6 us
    all_gather x2, blocking collectives, half_mixer(): lax.all_gather(hidden, 'kv', axis=0, tiled=True)  28.7 us
    reduce_scatter x1, waiting for transfers between devices, local(): lax.psum_scatter(jnp.concatenate([jnp.dot(normed, query_weight, preferred...  28.4 us
    all_gather x3, blocking collectives, gathered_norm(): gathered = lax.all_gather(shard, 'tp', axis=1, tiled=True)  26.4 us
    reduce_scatter x1, waiting for transfers between devices, local(): mixed = lax.psum_scatter(mixed_part, 'tp', scatter_dimension=1, tiled=True)  22.3 us
    all_gather x1, blocking collectives, local(): lax.all_gather(head_out, 'kv', axis=0, tiled=True)  14 us
  transfers between devices with their start and end apart: 6, of which 6 were waited for; matrix products, arithmetic and copies ran while one was open for 0% of the time, Pallas kernels for 0%

profile of v1, /device:TPU:0, one launch (start us, length us, event | category | flops | bytes accessed | tf_op | source)
XLA Modules:
  0.0 321.6 jit_solution(3656840878454320972)
XLA Ops:
  7.2 10.1 %all_gather.36 = bf16[64,512]{1,0:T(8,128)(2,1)S(1)} all-gather(bf16[64,128]{1,0:T(8,128)(2,1)} %param.19), channel_id=1, replica_groups=mesh['kv'=8,'tp'=4] {'tp'}, dimensions={1}, use_global_device_ids=true | all-gather | bytes 81920 | tf_op jit(solution)/shard_map/all_gather | solution.py:13
  17.3 0.1 fusion.8
  17.5 1.2 dynamic-slice
  19.4 0.2 dynamic-update-slice
  19.6 14.9 %all-reduce = f32[512]{0:T(512)S(1)} all-reduce(f32[512]{0:T(512)S(1)} %dynamic-update-slice), channel_id=2, replica_groups=mesh['kv'=8,'tp'=4] {'kv'}, use_global_device_ids=true, to_apply=%add | all-reduce | flops 512 | bytes 4096
  34.6 1.5 fusion.26
  36.1 0.3 copy-done.1
  36.4 0.7 fusion.24
  37.1 1.2 pad_maximum_fusion
  38.4 31.2 %reduce-scatter.7.cloned.1.call-done = f32[8,5632]{1,0:T(8,128)} async-done(((f32[64,5632]{1,0:T(8,128)}), f32[8,5632]{1,0:T(8,128)}) %reduce-scatter.7.cloned.1.call-update) | async-done | bytes 180240 | tf_op jit(solution)/shard_map/reduce_scatter | solution.py:23
  69.6 1.0 fusion.19
  70.6 14.4 %all_gather.39 = bf16[64,2816]{1,0:T(8,128)(2,1)S(1)} all-gather(bf16[8,2816]{1,0:T(8,128)(2,1)S(1)} %fusion.19), channel_id=1, replica_groups=mesh['kv'=8,'tp'=4] {'kv'}, dimensions={0}, use_global_device_ids=true | all-gather | bytes 405504 | tf_op jit(solution)/shard_map/all_gather | solution.py:37
  85.0 3.1 fusion.45
  88.1 22.3 %reduce-scatter.9.cloned.1.call-done = f32[64,128]{1,0:T(8,128)} async-done(((f32[64,512]{1,0:T(8,128)}), f32[64,128]{1,0:T(8,128)}) %reduce-scatter.9.cloned.1.call-update) | async-done | bytes 32784 | tf_op jit(solution)/shard_map/reduce_scatter | solution.py:41
  110.4 0.8 add_convert_fusion.1
  111.1 8.1 %all_gather.40 = bf16[64,512]{1,0:T(8,128)(2,1)S(1)} all-gather(bf16[64,128]{1,0:T(8,128)(2,1)S(1)} %add_convert_fusion.1), channel_id=1, replica_groups=mesh['kv'=8,'tp'=4] {'tp'}, dimensions={1}, use_global_device_ids=true | all-gather | bytes 81920 | tf_op jit(solution)/shard_map/all_gather | solution.py:13
  119.4 0.2 dynamic-update-slice.1
  119.6 13.8 %all-reduce.1 = f32[512]{0:T(512)S(1)} all-reduce(f32[512]{0:T(512)S(1)} %dynamic-update-slice.1), channel_id=3, replica_groups=mesh['kv'=8,'tp'=4] {'kv'}, use_global_device_ids=true, to_apply=%add.1 | all-reduce | flops 512 | bytes 4096
  133.6 1.3 fusion.42
  134.9 1.3 fusion.40
  136.2 1.3 fusion.38
  137.5 1.3 fusion.36
  138.8 0.8 pad_maximum_fusion.2
  139.9 28.4 %reduce-scatter.11.cloned.1.call-done = f32[8,2048]{1,0:T(8,128)} async-done(((f32[64,2048]{1,0:T(8,128)}), f32[8,2048]{1,0:T(8,128)}) %reduce-scatter.11.cloned.1.call-update) | async-done | bytes 65552 | tf_op jit(solution)/shard_map/reduce_scatter | solution.py:72
  168.3 0.8 fusion.33
  169.3 0.8 fusion
  170.1 1.1 fusion.17
  171.1 1.5 fusion.1
  172.6 1.3 multiply_add_fusion
  173.9 0.8 copy-done.4
  174.7 0.5 fusion.46
  175.4 0.8 fusion.30
  176.2 14.0 %all_gather.43 = bf16[64,512]{1,0:T(8,128)(2,1)S(1)} all-gather(bf16[8,512]{1,0:T(8,128)(2,1)S(1)} %fusion.30), channel_id=1, replica_groups=mesh['kv'=8,'tp'=4] {'kv'}, dimensions={0}, use_global_device_ids=true | all-gather | bytes 73728 | tf_op jit(solution)/shard_map/all_gather | solution.py:125
  190.2 0.8 fusion.47
  191.1 22.3 %reduce-scatter.13.cloned.1.call-done = f32[64,128]{1,0:T(8,128)} async-done(((f32[64,512]{1,0:T(8,128)}), f32[64,128]{1,0:T(8,128)}) %reduce-scatter.13.cloned.1.call-update) | async-done | bytes 32784 | tf_op jit(solution)/shard_map/reduce_scatter | solution.py:129
  213.4 0.8 add_convert_fusion
  214.2 8.1 %all_gather.44 = bf16[64,512]{1,0:T(8,128)(2,1)S(1)} all-gather(bf16[64,128]{1,0:T(8,128)(2,1)S(1)} %add_convert_fusion), channel_id=1, replica_groups=mesh['kv'=8,'tp'=4] {'tp'}, dimensions={1}, use_global_device_ids=true | all-gather | bytes 81920 | tf_op jit(solution)/shard_map/all_gather | solution.py:13
  222.4 0.2 dynamic-update-slice.2
  222.7 13.8 %all-reduce.2 = f32[512]{0:T(512)S(1)} all-reduce(f32[512]{0:T(512)S(1)} %dynamic-update-slice.2), channel_id=4, replica_groups=mesh['kv'=8,'tp'=4] {'kv'}, use_global_device_ids=true, to_apply=%add.2 | all-reduce | flops 512 | bytes 4096
  236.7 2.6 fusion.22
  239.3 0.7 fusion.20
  240.0 1.2 pad_maximum_fusion.1
  241.3 31.3 %reduce-scatter.15.cloned.1.call-done = f32[8,5632]{1,0:T(8,128)} async-done(((f32[64,5632]{1,0:T(8,128)}), f32[8,5632]{1,0:T(8,128)}) %reduce-scatter.15.cloned.1.call-update) | async-done | bytes 180240 | tf_op jit(solution)/shard_map/reduce_scatter | solution.py:23
  272.6 1.0 fusion.18
  273.5 14.4 %all_gather.47 = bf16[64,2816]{1,0:T(8,128)(2,1)S(1)} all-gather(bf16[8,2816]{1,0:T(8,128)(2,1)S(1)} %fusion.18), channel_id=1, replica_groups=mesh['kv'=8,'tp'=4] {'kv'}, dimensions={0}, use_global_device_ids=true | all-gather | bytes 405504 | tf_op jit(solution)/shard_map/all_gather | solution.py:37
  287.9 3.1 fusion.48
  291.2 22.2 %reduce-scatter.17.cloned.1.call-done = f32[64,128]{1,0:T(8,128)} async-done(((f32[64,512]{1,0:T(8,128)}), f32[64,128]{1,0:T(8,128)}) %reduce-scatter.17.cloned.1.call-update) | async-done | bytes 32784 | tf_op jit(solution)/shard_map/reduce_scatter | solution.py:41
  313.4 1.4 multiply_convert_fusion
  (67 shorter events, 1.7 us)
Async XLA Ops:
  7.2 27.4 %copy-start = (bf16[512,2816]{1,0:T(8,128)(2,1)S(1)}, bf16[512,2816]{1,0:T(8,128)(2,1)}, u32[]{:S(2)}) copy-start(bf16[512,2816]{1,0:T(8,128)(2,1)} %param.23) | copy-start | bytes 8650756
  7.2 28.9 %copy-start.8 = (f32[512]{0:T(512)S(1)}, f32[512]{0:T(512)}, u32[]{:S(2)}) copy-start(f32[512]{0:T(512)} %param.22) | copy-start | bytes 6148
  7.2 62.4 %reduce-scatter.7.cloned.1.call-start = ((), (), s32[]{:S(2)}) async-start(), calls=%async_computation.6 | async-start | bytes 1622016 | tf_op jit(solution)/shard_map/reduce_scatter | solution.py:23
  34.6 1.8 copy-start.1
  38.3 72.1 %copy-start.6 = (bf16[64,128]{1,0:T(8,128)(2,1)S(1)}, bf16[64,128]{1,0:T(8,128)(2,1)}, u32[]{:S(2)}) copy-start(bf16[64,128]{1,0:T(8,128)(2,1)} %param.19) | copy-start | bytes 49156
  38.3 95.3 %copy-start.7 = (f32[512]{0:T(512)S(1)}, f32[512]{0:T(512)}, u32[]{:S(2)}) copy-start(f32[512]{0:T(512)} %param.26) | copy-start | bytes 6148
  38.3 72.0 %reduce-scatter.9.cloned.1.call-start = ((), (), s32[]{:S(2)}) async-start(), calls=%async_computation.7 | async-start | bytes 163840 | tf_op jit(solution)/shard_map/reduce_scatter | solution.py:41
  88.0 51.6 %copy-start.12 = (s32[16]{0:T(128)S(1)}, s32[16]{0:T(128)}, u32[]{:S(2)}) copy-start(s32[16]{0:T(128)} %param.20) | copy-start | bytes 196
  88.0 51.9 %copy-start.11 = (f32[128]{0:T(128)S(1)}, f32[128]{0:T(128)}, u32[]{:S(2)}) copy-start(f32[128]{0:T(128)} %param.32) | copy-start | bytes 1540
  88.0 51.9 %copy-start.10 = (f32[512]{0:T(512)S(1)}, f32[512]{0:T(512)}, u32[]{:S(2)}) copy-start(f32[512]{0:T(512)} %param.31) | copy-start | bytes 6148
  88.0 81.2 %copy-start.3 = (f32[2,4,128,128]{3,2,1,0:T(8,128)S(1)}, f32[2,4,128,128]{3,2,1,0:T(8,128)}, u32[]{:S(2)}) copy-start(f32[2,4,128,128]{3,2,1,0:T(8,128)} %param.21) | copy-start | bytes 1572868
  88.1 80.2 %reduce-scatter.11.cloned.1.call-start = ((), (), s32[]{:S(2)}) async-start(), calls=%async_computation.8 | async-start | bytes 589824 | tf_op jit(solution)/shard_map/reduce_scatter | solution.py:72
  139.6 73.8 %reduce-scatter.13.cloned.1.call-start = ((), (), s32[]{:S(2)}) async-start(), calls=%async_computation.9 | async-start | bytes 163840 | tf_op jit(solution)/shard_map/reduce_scatter | solution.py:129
  169.1 21.1 %copy-start.5 = (bf16[512,512]{1,0:T(8,128)(2,1)S(1)}, bf16[512,512]{1,0:T(8,128)(2,1)}, u32[]{:S(2)}) copy-start(bf16[512,512]{1,0:T(8,128)(2,1)} %param.33) | copy-start | bytes 1572868
  169.3 67.4 %copy-start.9 = (f32[512]{0:T(512)S(1)}, f32[512]{0:T(512)}, u32[]{:S(2)}) copy-start(f32[512]{0:T(512)} %param.34) | copy-start | bytes 6148
  173.9 0.8 copy-start.4
  191.1 81.5 %reduce-scatter.15.cloned.1.call-start = ((), (), s32[]{:S(2)}) async-start(), calls=%async_computation.10 | async-start | bytes 1622016 | tf_op jit(solution)/shard_map/reduce_scatter | solution.py:23
  236.6 2.7 copy-start.2
  241.2 72.1 %reduce-scatter.17.cloned.1.call-start = ((), (), s32[]{:S(2)}) async-start(), calls=%async_computation.11 | async-start | bytes 163840 | tf_op jit(solution)/shard_map/reduce_scatter | solution.py:41
Sparse Core Ops, SparseCore 0:
  38.4 31.1 reduce-scatter.6
  88.2 22.1 reduce-scatter.8
  139.7 28.5 reduce-scatter.10
  191.2 22.1 reduce-scatter.12
  241.3 31.1 reduce-scatter.14
  291.1 22.1 reduce-scatter.16
